TPU v7x, 32 devices: a whole 2x2x4 slice. The times are simulated.
32 devices in a mesh: ep: 4 (over y, x), tp: 8 (over z, core).
Axes of the slice: x: 2, y: 2, z: 4, core: 2. Of those that a mesh axis runs over, the one named last changes fastest.
Arguments:
- tokens: bfloat16 [128, 4096], P('ep'), may hold values from -6 to 6
- norm_gain: float32 [4096], replicated, may hold values from 0.1 to 1.9
- group_ids: int32 [128, 1], P('ep'), may hold values from 0 to 1; in each aligned block of 32 rows (0 to 31, 32 to 63, ...) at most 32 rows name the same one
- local_ids: int32 [128, 4], P('ep'), may hold values from 0 to 7, all different within a row
- group_gate: float32 [128], P('ep'), may hold values from 0.3 to 1
- expert_gate: float32 [128, 4], P('ep'), may hold values from 0.1 to 1
- lengths: int32 [32], P('ep'), may hold values from 1 to 4, 64 in all
- w_gate: bfloat16 [16, 1024, 4096], P('ep', 'tp'), may hold values from -0.09375 to 0.09375
- w_up: bfloat16 [16, 1024, 4096], P('ep', 'tp'), may hold values from -0.09375 to 0.09375
- w_down: bfloat16 [16, 1024, 4096], P('ep', None, 'tp'), may hold values from -0.1875 to 0.1875
Outputs:
- mixed: bfloat16 [128, 4096], P('ep', 'tp')
Inputs may be any that keep to these rules, and one draw needn't show every extreme that they name: `group_ids`: among the 32 rows of one index of ep no group is named by more than 32 rows, and some index reaches 32. `local_ids`: each row names 4 different experts of its group. `lengths`: the first that many of a sequence's 4 positions are live.
All inputs are finite; a program needn't handle non-finite values. No bound on the sum of `lengths` on one device may be relied on, other than what follows from the above.
Results may differ from a plain program's by a relative error of at most 0.0065.
Values may be sent and summed in bfloat16 or wider, within the bound.
A program may use at most 64 MiB of HBM per device.

v0:
```python
import jax
import jax.numpy as jnp
from jax import lax
from jax.sharding import PartitionSpec as P

EXP_PER_GROUP = 8
STEP_TOK = 4


def norm_rows(tokens, norm_gain):
    values = tokens.astype(jnp.float32)
    scale = lax.rsqrt(jnp.mean(values * values, axis=1, keepdims=True) + 1e-06)
    return (values * scale * norm_gain).astype(jnp.bfloat16)


def live_mask(lengths, tok_rows):
    places = jnp.arange(tok_rows, dtype=jnp.int32)
    within = places % STEP_TOK
    owner = places // STEP_TOK
    seq_ids = jnp.arange(lengths.shape[0], dtype=jnp.int32)
    hits = (owner[:, None] == seq_ids[None, :]) & (within[:, None] < lengths[None, :])
    return jnp.any(hits, axis=1).astype(jnp.float32)


def expert_hidden(rows, w_gate, w_up):
    gate_part = jnp.einsum("rd,efd->ref", rows, w_gate, preferred_element_type=jnp.float32)
    up_part = jnp.einsum("rd,efd->ref", rows, w_up, preferred_element_type=jnp.float32)
    return (jax.nn.silu(gate_part) * up_part).astype(jnp.bfloat16)


def local(
    tokens, norm_gain, group_ids, local_ids, group_gate, expert_gate, lengths, w_gate, w_up, w_down
):
    highest = lax.Precision.HIGHEST
    tok_rows = tokens.shape[0]
    exp_dev = w_gate.shape[0]
    width_part = w_down.shape[2]
    ep_size = lax.axis_size("ep")
    groups = exp_dev * ep_size // EXP_PER_GROUP
    normed = norm_rows(tokens, norm_gain)
    live = live_mask(lengths, tok_rows)
    local_cols = jnp.arange(EXP_PER_GROUP, dtype=jnp.int32)
    picks = (local_ids[:, :, None] == local_cols[None, None, :]).astype(jnp.float32)
    weights = expert_gate * (group_gate * live)[:, None]
    dense = jnp.sum(picks * weights[:, :, None], axis=1)
    group_cols = jnp.arange(groups, dtype=jnp.int32)
    member_int = (group_ids == group_cols[None, :]).astype(jnp.int32)
    member = member_int.astype(jnp.float32)
    capacity = 2 * tok_rows // groups
    counts = jnp.cumsum(member_int, axis=0)
    rank = jnp.sum((counts - 1) * member_int, axis=1)
    slot_ids = jnp.arange(capacity, dtype=jnp.int32)
    select = member.T[:, None, :] * (rank[None, None, :] == slot_ids[None, :, None]).astype(
        jnp.float32
    )
    rows_by_group = jnp.einsum(
        "gct,td->gcd", select.astype(jnp.bfloat16), normed, preferred_element_type=jnp.float32
    ).astype(jnp.bfloat16)
    gates_by_group = jnp.einsum("gct,tl->gcl", select, dense, precision=highest)
    share = EXP_PER_GROUP // exp_dev
    send_rows = jnp.repeat(rows_by_group, share, axis=0)
    send_gates = gates_by_group.reshape(groups, capacity, share, exp_dev).transpose(0, 2, 1, 3)
    send_gates = send_gates.reshape(ep_size, capacity, exp_dev)
    recv_rows = lax.all_to_all(send_rows, "ep", split_axis=0, concat_axis=0, tiled=True)
    recv_gates = lax.all_to_all(send_gates, "ep", split_axis=0, concat_axis=0, tiled=True)
    slot_rows = recv_rows.reshape(ep_size * capacity, recv_rows.shape[2])
    slot_gates = recv_gates.reshape(ep_size * capacity, exp_dev)
    hidden = expert_hidden(slot_rows, w_gate, w_up)
    total = jnp.einsum(
        "ref,efd->red",
        lax.all_gather(hidden, "tp", axis=2, tiled=True),
        w_down,
        preferred_element_type=jnp.float32,
    )
    results = jnp.einsum("re,red->rd", slot_gates, total, precision=highest)
    results = results.reshape(ep_size, capacity, width_part)
    back = lax.all_to_all(results, "ep", split_axis=0, concat_axis=0, tiled=True)
    grouped = jnp.sum(back.reshape(groups, share, capacity, width_part), axis=1)
    mixed = jnp.einsum("gct,gcd->td", select, grouped, precision=highest)
    return mixed.astype(jnp.bfloat16)


def solution(mesh):
    in_specs = (
        P("ep", None),
        P(),
        P("ep", None),
        P("ep", None),
        P("ep"),
        P("ep", None),
        P("ep"),
        P("ep", "tp", None),
        P("ep", "tp", None),
        P("ep", None, "tp"),
    )
    out_specs = P("ep", "tp")
    return jax.shard_map(local, mesh=mesh, in_specs=in_specs, out_specs=out_specs, check_vma=False)
```

profile of v0, /device:TPU:0, one launch (start us, length us, event | category | flops | bytes accessed | tf_op | source)
XLA Modules:
  0.0 81.1 jit_solution(2347612556403566781)
XLA Ops:
  6.5 0.7 fusion.25
  7.2 0.7 fusion.17
  7.9 1.1 %fusion.4 = f32[32]{0:T(128)S(1)} fusion(bf16[32,4096]{1,0:T(8,128)(2,1)} %param.10), kind=kLoop, calls=%fused_computation.10 | loop fusion | flops 393184 | bytes 262272 | tf_op jit(solution)/shard_map/reduce_sum | solution.py:12
  9.1 1.0 %select_reduce_fusion.1 = s32[32]{0:T(128)S(1)} fusion(s32[32,2]{1,0:T(8,128)S(1)} %reduce_window_sum.11, s32[32]{0:T(128)} %bitcast.46), kind=kLoop, calls=%fused_computation.27 | loop fusion | flops 224 | bytes 512 | tf_op jit(solution)/shard_map/reduce_sum | solution.py:51
  10.2 1.6 %convolution_convert_fusion = bf16[2,32,4096]{2,1,0:T(8,128)(2,1)S(1)} fusion(bf16[32,4096]{1,0:T(8,128)(2,1)} %param.10, f32[4096]{0:T(1024)} %param.11, f32[32]{0:T(128)S(1)} %add_rsqrt_fusion, f32[32,32]{0,1:T(8,128)S(1)} %fusion.21, f32[2,32]{1,0:T(2,128)S(1)} %fusion.25), kind=kOutput, calls=%fused_computation | convolution fusion | flops 17567744 | bytes 807296 | tf_op jit(solution)/shard_map/gct,td->gcd/dot_general | solution.py:56
  11.7 0.1 broadcast_in_dim.2
  11.8 19.4 %all_to_all.15 = bf16[4,32,4096]{2,1,0:T(8,128)(2,1)S(1)} all-to-all(bf16[4,32,4096]{2,1,0:T(8,128)(2,1)S(1)} %bitcast.37), channel_id=1, replica_groups=mesh['ep'=4,'tp'=8] {'ep'}, dimensions={0} | all-to-all | bytes 2097152 | tf_op jit(solution)/shard_map/all_to_all | solution.py:64
  31.3 1.5 %fusion.27 = f32[128,4,128]{2,0,1:T(8,128)S(1)} fusion(bf16[128,4096,1]{1,0,2:T(8,128)(2,1)S(1)} %bitcast.38, bf16[4,128,4096]{2,1,0:T(8,128)(2,1)S(1)} %copy-done), kind=kOutput, calls=%fused_computation.51 | convolution fusion | flops 536870912 | bytes 5505024 | tf_op jit(solution)/shard_map/rd,efd->ref/dot_general | solution.py:26
  32.8 2.2 %fusion = bf16[128,4,128]{2,0,1:T(8,128)(2,1)} fusion(bf16[128,4096,1]{1,0,2:T(8,128)(2,1)S(1)} %bitcast.39, bf16[4,128,4096]{2,1,0:T(8,128)(2,1)S(1)} %copy-done.4, f32[128,4,128]{2,0,1:T(8,128)S(1)} %fusion.27), kind=kOutput, calls=%fused_computation.3 | convolution fusion | flops 537264128 | bytes 5636096 | tf_op jit(solution)/shard_map/rd,efd->ref/dot_general | solution.py:27
  35.1 0.1 fusion.24
  35.2 0.2 fusion.12
  35.4 0.1 pad_maximum_fusion
  35.5 0.1 reshape.102
  35.6 0.1 reshape.115
  35.7 7.0 %all_to_all.16 = f32[4,1,128]{2,1,0:T(1,128)S(1)} all-to-all(f32[4,1,128]{2,1,0:T(1,128)S(1)} %reshape.115), channel_id=1, replica_groups=mesh['ep'=4,'tp'=8] {'ep'}, dimensions={0} | all-to-all | bytes 4096 | tf_op jit(solution)/shard_map/all_to_all | solution.py:65
  42.7 0.5 broadcast.120
  43.2 0.7 reduce
  43.9 0.1 reshape.116
  44.0 0.1 copy.43
  44.1 14.7 %all-gather.2.cloned.1.call-done = bf16[128,4,1024]{2,0,1:T(8,128)(2,1)} async-done(((bf16[128,4,128]{2,0,1:T(8,128)(2,1)}), bf16[128,4,1024]{2,0,1:T(8,128)(2,1)}) %all-gather.2.cloned.1.call-update) | async-done | bytes 1048592 | tf_op jit(solution)/shard_map/all_gather | solution.py:71
  58.8 3.2 %convolution_bitcast_fusion = f32[128,4,512]{2,0,1:T(8,128)S(1)} fusion(bf16[128,4,1024]{2,0,1:T(8,128)(2,1)} %all-gather.2.cloned.1.call-done, bf16[4,1024,512]{2,1,0:T(8,128)(2,1)} %param.19), kind=kOutput, calls=%fused_computation.1 | convolution fusion | flops 536870912 | bytes 6291456 | tf_op jit(solution)/shard_map/ref,efd->red/dot_general | solution.py:69
  62.0 2.4 %fusion.2 = f32[128,1,512]{2,1,0:T(1,128)S(1)} fusion(f32[128,4,1]{1,2,0:T(1,128)S(1)} %bitcast.41, f32[128,4,512]{2,0,1:T(8,128)S(1)} %convolution_bitcast_fusion), kind=kOutput, calls=%fused_computation.6 | convolution fusion | flops 3145728 | bytes 1312768 | tf_op jit(solution)/shard_map/re,red->rd/dot_general | solution.py:75
  64.5 8.8 %all_to_all.17 = f32[4,32,512]{2,1,0:T(8,128)S(1)} all-to-all(f32[4,32,512]{2,1,0:T(8,128)S(1)} %bitcast.40), channel_id=1, replica_groups=mesh['ep'=4,'tp'=8] {'ep'}, dimensions={0} | all-to-all | bytes 524288 | tf_op jit(solution)/shard_map/all_to_all | solution.py:77
  73.3 0.9 %fusion.1 = bf16[32,512]{1,0:T(8,128)(2,1)} fusion(f32[2,32,512]{2,1,0:T(8,128)S(1)} %bitcast_reduce_fusion, f32[32,32]{0,1:T(8,128)S(1)} %fusion.21, f32[2,32]{1,0:T(2,128)S(1)} %fusion.25), kind=kOutput, calls=%fused_computation.5 | convolution fusion | flops 12601344 | bytes 168192 | tf_op jit(solution)/shard_map/gct,gcd->td/dot_general | solution.py:79
  (26 shorter events, 0.3 us)
Async XLA Ops:
  6.5 52.3 %all-gather.2.cloned.1.call-start = ((), (), s32[]{:S(2)}) async-start(), calls=%async_computation.3 | async-start | bytes 1179648 | tf_op jit(solution)/shard_map/all_gather | solution.py:71
  9.1 22.2 %copy-start = (bf16[4,128,4096]{2,1,0:T(8,128)(2,1)S(1)}, bf16[4,128,4096]{2,1,0:T(8,128)(2,1)}, u32[]{:S(2)}) copy-start(bf16[4,128,4096]{2,1,0:T(8,128)(2,1)} %param.17) | copy-start | bytes 12582916
  11.8 21.0 %copy-start.4 = (bf16[4,128,4096]{2,1,0:T(8,128)(2,1)S(1)}, bf16[4,128,4096]{2,1,0:T(8,128)(2,1)}, u32[]{:S(2)}) copy-start(bf16[4,128,4096]{2,1,0:T(8,128)(2,1)} %param.18) | copy-start | bytes 12582916
  32.8 2.3 %copy-start.3 = (s32[8]{0:T(128)S(1)}, s32[8]{0:T(128)}, u32[]{:S(2)}) copy-start(s32[8]{0:T(128)} %param.16) | copy-start | bytes 100
  32.8 2.4 %copy-start.5 = (f32[32]{0:T(128)S(1)}, f32[32]{0:T(128)}, u32[]{:S(2)}) copy-start(f32[32]{0:T(128)} %param.14) | copy-start | bytes 388
  32.8 2.4 %copy-start.1 = (f32[32,4]{0,1:T(4,128)S(1)}, f32[32,4]{0,1:T(4,128)}, u32[]{:S(2)}) copy-start(f32[32,4]{0,1:T(4,128)} %param.15) | copy-start | bytes 1540
  32.8 2.4 %copy-start.2 = (s32[32,4]{0,1:T(4,128)S(1)}, s32[32,4]{0,1:T(4,128)}, u32[]{:S(2)}) copy-start(s32[32,4]{0,1:T(4,128)} %param.13) | copy-start | bytes 1540
Sparse Core Ops, SparseCore 0:
  35.2 23.5 all-gather.1
where the time goes:
time: 81.4 us; the launch traced here: 81.1 us
  blocking collectives  35.2 us (43%)
  waiting for transfers between devices  14.7 us (18%)
  between operations  13.6 us (17%)
  matrix products  12.1 us (15%)
  other arithmetic  4.48 us (6%)
  local copies, waits for them, and re-layouts  1.06 us (1%)
    all_to_all x1, blocking collectives, local(): lax.all_to_all(send_rows, 'ep', split_axis=0, concat_axis=0, tiled=True)  19.4 us
    all_gather x1, waiting for transfers between devices, local(): lax.all_gather(hidden, 'tp', axis=2, tiled=True)  14.7 us
    all_to_all x1, blocking collectives, local(): lax.all_to_all(results, 'ep', split_axis=0, concat_axis=0, tiled=True)  8.79 us
    all_to_all x1, blocking collectives, local(): lax.all_to_all(send_gates, 'ep', split_axis=0, concat_axis=0, tiled=True)  7.01 us
    dot_general x1, matrix products, local(): jnp.einsum('ref,efd->red', lax.all_gather(hidden, 'tp', axis=2, tiled=Tru...  3.23 us
    dot_general x1, matrix products, local(): results = jnp.einsum('re,red->rd', slot_gates, total, precision=highest)  2.43 us
    dot_general x1, matrix products, expert_hidden(): jnp.einsum('rd,efd->ref', rows, w_up, preferred_element_type=jnp.float32)  2.18 us
  transfers between devices with their start and end apart: 1, of which 1 were waited for; matrix products, arithmetic and copies ran while one was open for 2% of the time, Pallas kernels for 0%

commit v1 on v0

--- a/solution.py
+++ b/solution.py
@@ -68,7 +68,7 @@
     hidden = expert_hidden(slot_rows, w_gate, w_up)
     total = jnp.einsum(
         "ref,efd->red",
-        lax.all_gather(hidden, "tp", axis=2, tiled=True),
+        jnp.concatenate(lax.all_gather(hidden, "tp"), axis=2),
         w_down,
         preferred_element_type=jnp.float32,
     )

time: 81.4 us -> 81.9 us (level)
  local copies, waits for them, and re-layouts: 1.06 us -> 2.67 us
  waiting for transfers between devices: 14.7 us -> 13.1 us
    all_gather x1, waiting for transfers between devices: 14.7 us -> 13.1 us  [local(): lax.all_gather(hidden, 'tp')]
    all_gather x0 -> x1, local copies, waits for them, and re-layouts: none -> 1.61 us  [local(): lax.all_gather(hidden, 'tp')]
where the time goes in v1:
time: 81.9 us; the launch traced here: 81.6 us
  blocking collectives  36 us (44%)
  between operations  13.6 us (17%)
  waiting for transfers between devices  13.1 us (16%)
  matrix products  11.8 us (14%)
  other arithmetic  4.48 us (5%)
  local copies, waits for them, and re-layouts  2.67 us (3%)
    all_to_all x1, blocking collectives, local(): lax.all_to_all(send_rows, 'ep', split_axis=0, concat_axis=0, tiled=True)  19.4 us
    all_gather x1, waiting for transfers between devices, local(): lax.all_gather(hidden, 'tp')  13.1 us
    all_to_all x1, blocking collectives, local(): lax.all_to_all(results, 'ep', split_axis=0, concat_axis=0, tiled=True)  9.58 us
    all_to_all x1, blocking collectives, local(): lax.all_to_all(send_gates, 'ep', split_axis=0, concat_axis=0, tiled=True)  7.01 us
    dot_general x1, matrix products, local(): jnp.einsum('ref,efd->red', jnp.concatenate(lax.all_gather(hidden, 'tp'),...  2.99 us
    dot_general x1, matrix products, local(): results = jnp.einsum('re,red->rd', slot_gates, total, precision=highest)  2.42 us
    dot_general x1, matrix products, expert_hidden(): jnp.einsum('rd,efd->ref', rows, w_up, preferred_element_type=jnp.float32)  2.18 us
  transfers between devices with their start and end apart: 1, of which 1 were waited for; matrix products, arithmetic and copies ran while one was open for 2% of the time, Pallas kernels for 0%

profile of v1, /device:TPU:0, one launch (start us, length us, event | category | flops | bytes accessed | tf_op | source)
XLA Modules:
  0.0 81.6 jit_solution(1017924528406726188)
XLA Ops:
  6.5 0.7 fusion.25
  7.2 0.7 fusion.17
  7.9 1.1 %fusion.4 = f32[32]{0:T(128)S(1)} fusion(bf16[32,4096]{1,0:T(8,128)(2,1)} %param.10), kind=kLoop, calls=%fused_computation.10 | loop fusion | flops 393184 | bytes 262272 | tf_op jit(solution)/shard_map/reduce_sum | solution.py:12
  9.1 1.0 %select_reduce_fusion.1 = s32[32]{0:T(128)S(1)} fusion(s32[32,2]{1,0:T(8,128)S(1)} %reduce_window_sum.11, s32[32]{0:T(128)} %bitcast.52), kind=kLoop, calls=%fused_computation.27 | loop fusion | flops 224 | bytes 512 | tf_op jit(solution)/shard_map/reduce_sum | solution.py:51
  10.2 1.6 %convolution_convert_fusion = bf16[2,32,4096]{2,1,0:T(8,128)(2,1)S(1)} fusion(bf16[32,4096]{1,0:T(8,128)(2,1)} %param.10, f32[4096]{0:T(1024)} %param.11, f32[32]{0:T(128)S(1)} %add_rsqrt_fusion, f32[32,32]{0,1:T(8,128)S(1)} %fusion.21, f32[2,32]{1,0:T(2,128)S(1)} %fusion.25), kind=kOutput, calls=%fused_computation | convolution fusion | flops 17567744 | bytes 807296 | tf_op jit(solution)/shard_map/gct,td->gcd/dot_general | solution.py:56
  11.7 0.1 broadcast_in_dim.2
  11.8 19.4 %all_to_all.15 = bf16[4,32,4096]{2,1,0:T(8,128)(2,1)S(1)} all-to-all(bf16[4,32,4096]{2,1,0:T(8,128)(2,1)S(1)} %bitcast.42), channel_id=1, replica_groups=mesh['ep'=4,'tp'=8] {'ep'}, dimensions={0} | all-to-all | bytes 2097152 | tf_op jit(solution)/shard_map/all_to_all | solution.py:64
  31.3 1.5 %fusion.27 = f32[128,4,128]{2,0,1:T(8,128)S(1)} fusion(bf16[128,4096,1]{1,0,2:T(8,128)(2,1)S(1)} %bitcast.43, bf16[4,128,4096]{2,1,0:T(8,128)(2,1)S(1)} %copy-done), kind=kOutput, calls=%fused_computation.51 | convolution fusion | flops 536870912 | bytes 5505024 | tf_op jit(solution)/shard_map/rd,efd->ref/dot_general | solution.py:26
  32.8 2.2 %fusion = bf16[128,4,128]{2,0,1:T(8,128)(2,1)} fusion(bf16[128,4096,1]{1,0,2:T(8,128)(2,1)S(1)} %bitcast.44, bf16[4,128,4096]{2,1,0:T(8,128)(2,1)S(1)} %copy-done.4, f32[128,4,128]{2,0,1:T(8,128)S(1)} %fusion.27), kind=kOutput, calls=%fused_computation.3 | convolution fusion | flops 537264128 | bytes 5636096 | tf_op jit(solution)/shard_map/rd,efd->ref/dot_general | solution.py:27
  35.1 0.1 fusion.24
  35.2 0.2 fusion.12
  35.5 0.1 reshape.108
  35.6 0.1 reshape.124
  35.7 7.0 %all_to_all.16 = f32[4,1,128]{2,1,0:T(1,128)S(1)} all-to-all(f32[4,1,128]{2,1,0:T(1,128)S(1)} %reshape.124), channel_id=1, replica_groups=mesh['ep'=4,'tp'=8] {'ep'}, dimensions={0} | all-to-all | bytes 4096 | tf_op jit(solution)/shard_map/all_to_all | solution.py:65
  42.7 0.5 broadcast.120
  43.2 0.7 reduce
  43.9 0.1 reshape.125
  44.0 0.1 copy.51
  44.1 13.1 %all-gather.3.cloned.1.call-done = bf16[1024,4,128]{2,0,1:T(8,128)(2,1)} async-done(((bf16[128,4,128]{2,0,1:T(8,128)(2,1)}), bf16[1024,4,128]{2,0,1:T(8,128)(2,1)}) %all-gather.3.cloned.1.call-update) | async-done | bytes 1048592 | tf_op jit(solution)/shard_map/all_gather | solution.py:71
  57.2 1.6 %copy.43 = bf16[8,128,4,128]{1,3,0,2:T(8,128)(2,1)S(1)} copy(bf16[8,128,4,128]{3,1,0,2:T(8,128)(2,1)} %bitcast.45) | data formatting | bytes 2097152 | tf_op jit(solution)/shard_map/all_gather | solution.py:71
  58.8 3.0 %convolution_bitcast_fusion = f32[128,4,512]{2,0,1:T(8,128)S(1)} fusion(bf16[128,4,1024]{0,2,1:T(8,128)(2,1)S(1)} %bitcast.41, bf16[4,1024,512]{2,1,0:T(8,128)(2,1)} %param.19), kind=kOutput, calls=%fused_computation.1 | convolution fusion | flops 536870912 | bytes 6291456 | tf_op jit(solution)/shard_map/ref,efd->red/dot_general | solution.py:69
  61.8 2.4 %fusion.2 = f32[128,1,512]{2,1,0:T(1,128)S(1)} fusion(f32[128,4,1]{1,2,0:T(1,128)S(1)} %bitcast.47, f32[128,4,512]{2,0,1:T(8,128)S(1)} %convolution_bitcast_fusion), kind=kOutput, calls=%fused_computation.6 | convolution fusion | flops 3145728 | bytes 1312768 | tf_op jit(solution)/shard_map/re,red->rd/dot_general | solution.py:75
  64.2 9.6 %all_to_all.17 = f32[4,32,512]{2,1,0:T(8,128)S(1)} all-to-all(f32[4,32,512]{2,1,0:T(8,128)S(1)} %bitcast.46), channel_id=1, replica_groups=mesh['ep'=4,'tp'=8] {'ep'}, dimensions={0} | all-to-all | bytes 524288 | tf_op jit(solution)/shard_map/all_to_all | solution.py:77
  73.8 0.9 %fusion.1 = bf16[32,512]{1,0:T(8,128)(2,1)} fusion(f32[2,32,512]{2,1,0:T(8,128)S(1)} %bitcast_reduce_fusion, f32[32,32]{0,1:T(8,128)S(1)} %fusion.21, f32[2,32]{1,0:T(2,128)S(1)} %fusion.25), kind=kOutput, calls=%fused_computation.5 | convolution fusion | flops 12601344 | bytes 168192 | tf_op jit(solution)/shard_map/gct,gcd->td/dot_general | solution.py:79
  (27 shorter events, 0.3 us)
Async XLA Ops:
  6.5 50.6 %all-gather.3.cloned.1.call-start = ((), (), s32[]{:S(2)}) async-start(), calls=%async_computation.3 | async-start | bytes 1179648 | tf_op jit(solution)/shard_map/all_gather | solution.py:71
  9.1 22.2 %copy-start = (bf16[4,128,4096]{2,1,0:T(8,128)(2,1)S(1)}, bf16[4,128,4096]{2,1,0:T(8,128)(2,1)}, u32[]{:S(2)}) copy-start(bf16[4,128,4096]{2,1,0:T(8,128)(2,1)} %param.17) | copy-start | bytes 12582916
  11.8 21.0 %copy-start.4 = (bf16[4,128,4096]{2,1,0:T(8,128)(2,1)S(1)}, bf16[4,128,4096]{2,1,0:T(8,128)(2,1)}, u32[]{:S(2)}) copy-start(bf16[4,128,4096]{2,1,0:T(8,128)(2,1)} %param.18) | copy-start | bytes 12582916
  32.8 2.3 %copy-start.3 = (s32[8]{0:T(128)S(1)}, s32[8]{0:T(128)}, u32[]{:S(2)}) copy-start(s32[8]{0:T(128)} %param.16) | copy-start | bytes 100
  32.8 2.4 %copy-start.5 = (f32[32]{0:T(128)S(1)}, f32[32]{0:T(128)}, u32[]{:S(2)}) copy-start(f32[32]{0:T(128)} %param.14) | copy-start | bytes 388
  32.8 2.4 %copy-start.1 = (f32[32,4]{0,1:T(4,128)S(1)}, f32[32,4]{0,1:T(4,128)}, u32[]{:S(2)}) copy-start(f32[32,4]{0,1:T(4,128)} %param.15) | copy-start | bytes 1540
  32.8 2.4 %copy-start.2 = (s32[32,4]{0,1:T(4,128)S(1)}, s32[32,4]{0,1:T(4,128)}, u32[]{:S(2)}) copy-start(s32[32,4]{0,1:T(4,128)} %param.13) | copy-start | bytes 1540
Sparse Core Ops, SparseCore 0:
  35.2 21.9 all-gather.2
